TPU v7x, 32 devices: a whole 2x2x4 slice. The times are simulated.
32 devices in a mesh: grp: 2 (over y), ep: 16 (over z, x, core), tp: 1.
Axes of the slice: x: 2, y: 2, z: 4, core: 2. Of those that a mesh axis runs over, the one named last changes fastest.
Arguments:
- tokens: bfloat16 [2048, 2048], P(('grp', 'ep')), parts along dimension 0, may hold values from -6 to 6
- norm_gain: float32 [2048], replicated, may hold values from 0.1 to 1.9
- routes: int32 [2048, 6], P(('grp', 'ep')), parts along dimension 0, may hold values from 0 to 15, all different within a row; in each aligned block of 64 rows (0 to 63, 64 to 127, ...) at most 48 rows name the same one
- route_weights: float32 [2048, 6], P(('grp', 'ep')), parts along dimension 0, may hold values from 0.05 to 1
- w_gate: bfloat16 [16, 2048, 2048], P('ep', None, 'tp'), may hold values from -0.125 to 0.125
- w_up: bfloat16 [16, 2048, 2048], P('ep', None, 'tp'), may hold values from -0.125 to 0.125
- w_down: bfloat16 [16, 2048, 2048], P('ep', 'tp'), may hold values from -4 to 4
- final_gain: float32 [2048], P('tp'), may hold values from 0.1 to 1.9
Outputs:
- mixed_out: bfloat16 [2048, 2048], P(('grp', 'ep'), 'tp'), parts along dimension 0
There are 2 independent parts, one for each index of `grp`. A program takes and returns all parts, laid end to end along the dimension named above; an argument that names none is the same for every part. Nothing has to cross between parts.
Inputs may be any that keep to these rules, and one draw needn't show every extreme that they name: `routes`: each row names 6 different experts; within the rows of one index of ep no expert is named by more than 48 rows, and in every draw some expert is named by exactly 48 rows of some index.
All inputs are finite; a program needn't handle non-finite values.
Results may differ from a plain program's by a relative error of at most 0.015.
Values may be sent and summed in bfloat16 or wider, within the bound.
A program may use at most 64 MiB of HBM per device.

v0:
```python
import functools

import jax
import jax.numpy as jnp
from jax import lax
from jax.experimental import pallas as pl
from jax.experimental.pallas import tpu as pltpu
from jax.sharding import PartitionSpec as P

TOP_K = 6


EPS = 1e-06
MESH = pl.DeviceIdType.MESH


def slot_table(route_rows, experts_all, capacity):
    flattened = route_rows.reshape(-1)
    matches = (flattened[:, None] == jnp.arange(experts_all, dtype=jnp.int32)[None, :]).astype(
        jnp.int32
    )
    earlier = jnp.cumsum(matches, axis=0) - matches
    slot_of = jnp.sum(earlier * matches, axis=1)
    return (flattened * capacity + slot_of).reshape(route_rows.shape)


def per_device(tokens, norm_gain, routes, route_weights, w_gate, w_up, w_down, final_gain):
    tok_count, features = tokens.shape
    ep_size = lax.axis_size("ep")
    exp_local = w_gate.shape[0]
    experts_all = exp_local * ep_size
    capacity = max(2, min(tok_count, 2 * tok_count * TOP_K // experts_all))
    slot_count = experts_all * capacity
    tokens_f = tokens.astype(jnp.float32)
    inverse = lax.rsqrt(jnp.mean(tokens_f * tokens_f, axis=1, keepdims=True) + EPS)
    normed = (tokens_f * inverse * norm_gain[None, :]).astype(jnp.bfloat16)
    places = slot_table(routes, experts_all, capacity)
    slot_ids = jnp.arange(slot_count, dtype=jnp.int32)
    matched = places[:, :, None] == slot_ids[None, None, :]
    selector = jnp.sum(matched.astype(jnp.float32), axis=1).T.astype(jnp.bfloat16)
    combine_rows = jnp.sum(jnp.where(matched, route_weights[:, :, None], 0.0), axis=1)
    outgoing = jnp.dot(selector, normed, preferred_element_type=jnp.float32).astype(jnp.bfloat16)
    outgoing = outgoing.reshape(ep_size, exp_local, capacity, features)
    received = lax.all_to_all(outgoing, "ep", split_axis=0, concat_axis=0, tiled=True)
    gate_value = jnp.einsum("secd,edf->secf", received, w_gate, preferred_element_type=jnp.float32)
    up_value = jnp.einsum("secd,edf->secf", received, w_up, preferred_element_type=jnp.float32)
    hidden = (jax.nn.silu(gate_value) * up_value).astype(jnp.bfloat16)
    partial_value = jnp.einsum("secf,efd->secd", hidden, w_down, preferred_element_type=jnp.float32)
    summed = lax.psum_scatter(
        partial_value.astype(jnp.bfloat16), "tp", scatter_dimension=3, tiled=True
    )
    returned = lax.all_to_all(summed, "ep", split_axis=0, concat_axis=0, tiled=True)
    results = returned.reshape(slot_count, returned.shape[3]).astype(jnp.float32)
    combined = jnp.dot(combine_rows, results, precision=lax.Precision.HIGHEST)
    local_squares = jnp.sum(combined * combined, axis=1)
    squares_all = lax.psum(local_squares, "tp")
    inverse_out = lax.rsqrt(squares_all / features + EPS)
    return (combined * inverse_out[:, None] * final_gain[None, :]).astype(jnp.bfloat16)


def fused_kernel(nz, tile, tokens_ref, gain_ref, routes_ref, rw_ref, wg_hbm, wu_hbm, wd_hbm, fgain_ref,
                 out_ref, buf, wg, wu, wd, hid, part, dbuf, xbuf, zbuf, wsem,
                 az_s, az_r, ax_s, ax_r, ad_s, ad_r, rd_s, rd_r, rx_s, rx_r, rz_s, rz_r):
    rows, features = tokens_ref.shape
    hidden_units = wg.shape[1]
    experts = 4 * nz
    chunk = 4 * rows
    f32, bf16 = jnp.float32, jnp.bfloat16
    me = lax.axis_index("ep")
    core = lax.rem(me, 2)
    x = lax.rem(lax.div(me, 2), 2)
    z = lax.div(me, 4)
    d_peer = me + 1 - 2 * core
    x_peer = me + 2 - 4 * x

    def z_of(dz):
        return lax.rem(z + dz, nz)

    def z_peer(dz):
        return z_of(dz) * 4 + x * 2 + core

    def weight_copy(which, j):
        src, dst = ((wg_hbm, wg), (wu_hbm, wu), (wd_hbm, wd))[which]
        cols = pl.ds(pl.multiple_of(j * tile, tile), tile)
        return pltpu.make_async_copy(src.at[0, :, cols], dst.at[:, cols], wsem.at[which, j])

    gu_tiles, d_tiles = hidden_units // tile, features // tile
    for j in range(gu_tiles):
        weight_copy(0, j).start()
        weight_copy(1, j).start()
    for j in range(d_tiles):
        weight_copy(2, j).start()

    barrier = pltpu.get_barrier_semaphore()
    peers = [d_peer, x_peer] + [z_peer(dz) for dz in range(1, nz)]
    for peer in peers:
        pl.semaphore_signal(barrier, inc=1, device_id={"ep": peer}, device_id_type=MESH)

    own = pl.ds(pl.multiple_of(me * rows, rows), rows)
    tok = tokens_ref[...].astype(f32)
    inverse = lax.rsqrt(jnp.mean(tok * tok, axis=1, keepdims=True) + EPS)
    buf[own, :features] = (tok * inverse * gain_ref[...]).astype(bf16)
    extra = buf.shape[1] - features
    lanes = lax.broadcasted_iota(jnp.int32, (rows, extra), 1)
    first = jnp.zeros((rows, extra), f32)
    second = jnp.zeros((rows, extra), f32)
    for k in range(routes_ref.shape[1]):
        r, w = routes_ref[:, k:k + 1], rw_ref[:, k:k + 1]
        first = first + jnp.where(lanes == r, w, 0.0)
        second = second + jnp.where(lanes == r + experts, w, 0.0)
    rest = second - second.astype(bf16).astype(f32)
    buf[own, features:] = (first + rest).astype(bf16)

    pl.semaphore_wait(barrier, len(peers))

    def remote(src, dst, s, r, dev):
        return pltpu.make_async_remote_copy(
            src_ref=src, dst_ref=dst, send_sem=s, recv_sem=r, device_id={"ep": dev}, device_id_type=MESH
        )

    def block(e):
        return buf.at[pl.ds(pl.multiple_of(e * rows, rows), rows), :]

    own_step = nz - 1
    tables = [sorted((p for p in range(nz) if p != q), key=lambda p: (abs(p - q), p)) for q in range(nz)]
    places = []
    for i in range(own_step):
        value = tables[0][i]
        for q in range(1, nz):
            value = jnp.where(z == q, tables[q][i], value)
        places.append(value)
    places.append(z)

    def same_col(i):
        return block(places[i] * 4 + x * 2 + core)

    def other_col(i):
        return block(places[i] * 4 + (1 - x) * 2 + core)

    def ag_z(i, up):
        ref = same_col(i)
        peer = me + 4 if up else me - 4
        return remote(ref, ref, az_s.at[i, int(up)], az_r.at[places[i]], peer)

    def ag_x(i, arriving=False):
        ref = other_col(i) if arriving else same_col(i)
        return remote(ref, ref, ax_s.at[i], ax_r.at[i], x_peer)

    def ag_d(i, j, arriving=False):
        if arriving:
            col = x if j == 0 else 1 - x
            ref = block(places[i] * 4 + col * 2 + 1 - core)
        else:
            ref = same_col(i) if j == 0 else other_col(i)
        return remote(ref, ref, ad_s.at[i, j], ad_r.at[i, j], d_peer)

    def rs_block(i, same_x, same_core):
        col = x if same_x else 1 - x
        lane = core if same_core else 1 - core
        at = pl.multiple_of((col * 2 + lane) * rows, rows)
        return part.at[i, pl.ds(at, rows), :]

    def rs_d(i, j):
        return remote(rs_block(i, j == 0, False), dbuf.at[i, j], rd_s.at[i, j], rd_r.at[i, j], d_peer)

    def rs_x(i):
        return remote(rs_block(i, False, True), xbuf.at[i], rx_s.at[i], rx_r.at[i], x_peer)

    def rs_z(i):
        peer = places[i] * 4 + x * 2 + core
        return remote(rs_block(i, True, True), zbuf.at[z], rz_s.at[i], rz_r.at[z], peer)

    def rs_z_arriving(i):
        peer = places[i] * 4 + x * 2 + core
        ref = zbuf.at[places[i]]
        return remote(ref, ref, rz_s.at[i], rz_r.at[places[i]], peer)

    def pass_on(i, action):
        from_below, from_above = places[i] <= z, places[i] >= z

        @pl.when(jnp.logical_and(from_below, z < nz - 1))
        def _():
            action(ag_z(i, True))

        @pl.when(jnp.logical_and(from_above, z > 0))
        def _():
            action(ag_z(i, False))

    pass_on(own_step, lambda copy: copy.start())
    ag_x(own_step).start()
    ag_d(own_step, 0).start()

    def forward_z(i):
        ag_z(i, True).wait_recv()
        pass_on(i, lambda copy: copy.start())
        ag_x(i).start()
        ag_d(i, 0).start()

    def forward_x(i):
        ag_x(i, True).wait_recv()
        ag_d(i, 1).start()

    def chunk_rows(i):
        return pl.ds(pl.multiple_of(places[i] * chunk, chunk), chunk)

    def gate_up(i, begin, end, wait):
        here = chunk_rows(i)

        def body(j, carry):
            if wait:
                weight_copy(0, j).wait()
                weight_copy(1, j).wait()
            cols = pl.ds(pl.multiple_of(j * tile, tile), tile)
            lhs = buf[here, :features]
            g = jnp.dot(lhs, wg[:, cols], preferred_element_type=f32)
            u = jnp.dot(lhs, wu[:, cols], preferred_element_type=f32)
            hid[:, cols] = (g / (1.0 + jnp.exp(-g)) * u).astype(bf16)
            return carry

        lax.fori_loop(begin, end, body, 0)

    def down(i, begin, end, wait):
        ext = buf[chunk_rows(i), features:].astype(f32)
        lane = lax.broadcasted_iota(jnp.int32, ext.shape, 1)
        mine = jnp.logical_or(lane == me, lane == me + experts)
        weight = jnp.sum(jnp.where(mine, ext, 0.0), axis=1, keepdims=True)

        def body(j, carry):
            if wait:
                weight_copy(2, j).wait()
            cols = pl.ds(pl.multiple_of(j * tile, tile), tile)
            o = jnp.dot(hid[...], wd[:, cols], preferred_element_type=f32)
            part[i, :, cols] = (o * weight).astype(bf16)
            return carry

        lax.fori_loop(begin, end, body, 0)

    def finish_d(i):
        rs_d(i, 1).wait_recv()
        ref = rs_block(i, False, True)
        ref[...] = (ref[...].astype(f32) + dbuf[i, 1].astype(f32)).astype(bf16)
        rs_d(i, 0).wait_recv()
        rs_x(i).start()

    def finish_x(i):
        rs_x(i).wait_recv()
        ref = rs_block(i, True, True)
        total = ref[...].astype(f32) + dbuf[i, 0].astype(f32) + xbuf[i].astype(f32)
        if i == own_step:
            return total
        ref[...] = total.astype(bf16)
        rs_z(i).start()
        return None

    forward_z(0)
    forward_x(own_step)
    forward_z(1)
    forward_x(0)

    gu_half, d_half = max(1, gu_tiles // 2), max(1, d_tiles // 2)
    for i in range(nz):
        ag_d(i, 0, True).wait_recv()
        ag_d(i, 1, True).wait_recv()
        gate_up(i, 0, gu_half, i == 0)
        if i >= 1:
            finish_d(i - 1)
        gate_up(i, gu_half, gu_tiles, i == 0)
        down(i, 0, d_half, i == 0)
        if i + 1 < own_step:
            forward_x(i + 1)
        if i >= 2:
            finish_x(i - 2)
        down(i, d_half, d_tiles, i == 0)
        rs_d(i, 1).start()
        rs_d(i, 0).start()
        if i + 2 < own_step:
            forward_z(i + 2)

    finish_d(own_step)
    finish_x(own_step - 1)
    total = finish_x(own_step)
    for i in range(own_step):
        rs_z_arriving(i).wait_recv()
        total = total + zbuf[places[i]].astype(f32)
    inverse_out = lax.rsqrt(jnp.mean(total * total, axis=1, keepdims=True) + EPS)
    out_ref[...] = (total * inverse_out * fgain_ref[...]).astype(out_ref.dtype)

    for i in range(nz):
        pass_on(i, lambda copy: copy.wait_send())
        ag_x(i).wait_send()
        rs_x(i).wait_send()
        for j in range(2):
            ag_d(i, j).wait_send()
            rs_d(i, j).wait_send()
        if i < own_step:
            rs_z(i).wait_send()


def fused_device(tokens, norm_gain, routes, route_weights, w_gate, w_up, w_down, final_gain):
    rows, features = tokens.shape
    hidden_units = w_gate.shape[2]
    experts = lax.axis_size("ep")
    nz = experts // 4
    tile = 1024
    extra = -(-2 * experts // 128) * 128
    vmem, anywhere = pl.BlockSpec(memory_space=pltpu.VMEM), pl.BlockSpec(memory_space=pl.ANY)
    dma = pltpu.SemaphoreType.DMA
    bf16 = jnp.bfloat16
    tiles = max(hidden_units, features) // tile
    return pl.pallas_call(
        functools.partial(fused_kernel, nz, tile),
        out_shape=jax.ShapeDtypeStruct((rows, features), jnp.bfloat16),
        in_specs=[vmem, vmem, vmem, vmem, anywhere, anywhere, anywhere, vmem],
        out_specs=vmem,
        scratch_shapes=[
            pltpu.VMEM((experts * rows, features + extra), bf16),
            pltpu.VMEM((features, hidden_units), bf16),
            pltpu.VMEM((features, hidden_units), bf16),
            pltpu.VMEM((hidden_units, features), bf16),
            pltpu.VMEM((4 * rows, hidden_units), bf16),
            pltpu.VMEM((nz, 4 * rows, features), bf16),
            pltpu.VMEM((nz, 2, rows, features), bf16),
            pltpu.VMEM((nz, rows, features), bf16),
            pltpu.VMEM((nz, rows, features), bf16),
            dma((3, tiles)),
            dma((nz, 2)), dma((nz,)), dma((nz,)), dma((nz,)), dma((nz, 2)), dma((nz, 2)),
            dma((nz, 2)), dma((nz, 2)), dma((nz,)), dma((nz,)), dma((nz,)), dma((nz,)),
        ],
        compiler_params=pltpu.CompilerParams(
            collective_id=0, has_side_effects=True, vmem_limit_bytes=60 * 1024 * 1024
        ),
    )(tokens, norm_gain[None, :], routes, route_weights, w_gate, w_up, w_down, final_gain[None, :])


def solution(mesh):
    placed = (
        P(("grp", "ep"), None),
        P(),
        P(("grp", "ep"), None),
        P(("grp", "ep"), None),
        P("ep", None, "tp"),
        P("ep", None, "tp"),
        P("ep", "tp", None),
        P("tp"),
    )
    ep, tp = mesh.shape["ep"], mesh.shape["tp"]

    def step(*args):
        rows, features = args[0].shape
        hidden_units = args[4].shape[2]
        fits = 3 * features * hidden_units + 3 * ep * rows * features < 24 * 2 ** 20
        whole_tiles = features % 1024 == 0 and hidden_units % 1024 == 0 and rows % 16 == 0
        if tp == 1 and ep % 4 == 0 and ep >= 12 and args[4].shape[0] == 1 and fits and whole_tiles:
            return fused_device(*args)
        return per_device(*args)

    return jax.shard_map(
        step, mesh=mesh, in_specs=placed, out_specs=P(("grp", "ep"), "tp"), check_vma=False
    )
```

profile of v0, /device:TPU:0, one launch (start us, length us, event | category | flops | bytes accessed | tf_op | source)
XLA Modules:
  0.0 82.5 jit_solution(8758753401535222895)
XLA Ops:
  0.0 1.4 %copy.9.routes_ref = s32[64,6]{1,0:T(8,128)} copy(s32[64,6]{0,1:T(8,128)} %param.10) | data formatting | bytes 3072 | tf_op args[2]
  1.4 1.4 %copy.10.rw_ref = f32[64,6]{1,0:T(8,128)} copy(f32[64,6]{0,1:T(8,128)} %param.11) | data formatting | bytes 3072 | tf_op args[3]
  2.8 78.0 %shard_map.82 = bf16[64,2048]{1,0:T(8,128)(2,1)} custom-call(bf16[64,2048]{1,0:T(8,128)(2,1)} %tokens_ref.1, f32[1,2048]{1,0:T(1,128)} %bitcast.2, s32[64,6]{1,0:T(8,128)} %copy.9.routes_ref, f32[64,6]{1,0:T(8,128)} %copy.10.rw_ref, bf16[1,2048,2048]{2,1,0:T(8,128)(2,1)} %wg_hbm.1, bf16[1,2048,2048]{2,1,0:T(8,128)(2,1)} %wu_hbm.1, ...), custom_call_target="tpu_custom_call" | custom-call | tf_op jit(solution)/shard_map/pallas_call | solution.py:310
  80.8 1.7 %copy.12 = bf16[64,2048]{1,0:T(8,128)(2,1)} copy(bf16[64,2048]{1,0:T(8,128)(2,1)} %shard_map.82) | data formatting | bytes 524288
where the time goes:
time: 82.7 us; the launch traced here: 82.5 us
  Pallas kernels  78 us (94%)
  local copies, waits for them, and re-layouts  4.43 us (5%)
    pallas_call x1, Pallas kernels, fused_device(): pl.pallas_call(functools.partial(fused_kernel, nz, tile), out_shape=jax.S...  78 us
    unnamed x3, local copies, waits for them, and re-layouts  4.43 us

commit v1 on v0

v1 whole, which is shorter than its diff:
```python
import functools

import jax
import jax.numpy as jnp
from jax import lax
from jax.experimental import pallas as pl
from jax.experimental.pallas import tpu as pltpu
from jax.sharding import PartitionSpec as P

TOP_K = 6


EPS = 1e-06
MESH = pl.DeviceIdType.MESH
META = None


def slot_table(route_rows, experts_all, capacity):
    flattened = route_rows.reshape(-1)
    matches = (flattened[:, None] == jnp.arange(experts_all, dtype=jnp.int32)[None, :]).astype(
        jnp.int32
    )
    earlier = jnp.cumsum(matches, axis=0) - matches
    slot_of = jnp.sum(earlier * matches, axis=1)
    return (flattened * capacity + slot_of).reshape(route_rows.shape)


def per_device(tokens, norm_gain, routes, route_weights, w_gate, w_up, w_down, final_gain):
    tok_count, features = tokens.shape
    ep_size = lax.axis_size("ep")
    exp_local = w_gate.shape[0]
    experts_all = exp_local * ep_size
    capacity = max(2, min(tok_count, 2 * tok_count * TOP_K // experts_all))
    slot_count = experts_all * capacity
    tokens_f = tokens.astype(jnp.float32)
    inverse = lax.rsqrt(jnp.mean(tokens_f * tokens_f, axis=1, keepdims=True) + EPS)
    normed = (tokens_f * inverse * norm_gain[None, :]).astype(jnp.bfloat16)
    places = slot_table(routes, experts_all, capacity)
    slot_ids = jnp.arange(slot_count, dtype=jnp.int32)
    matched = places[:, :, None] == slot_ids[None, None, :]
    selector = jnp.sum(matched.astype(jnp.float32), axis=1).T.astype(jnp.bfloat16)
    combine_rows = jnp.sum(jnp.where(matched, route_weights[:, :, None], 0.0), axis=1)
    outgoing = jnp.dot(selector, normed, preferred_element_type=jnp.float32).astype(jnp.bfloat16)
    outgoing = outgoing.reshape(ep_size, exp_local, capacity, features)
    received = lax.all_to_all(outgoing, "ep", split_axis=0, concat_axis=0, tiled=True)
    gate_value = jnp.einsum("secd,edf->secf", received, w_gate, preferred_element_type=jnp.float32)
    up_value = jnp.einsum("secd,edf->secf", received, w_up, preferred_element_type=jnp.float32)
    hidden = (jax.nn.silu(gate_value) * up_value).astype(jnp.bfloat16)
    partial_value = jnp.einsum("secf,efd->secd", hidden, w_down, preferred_element_type=jnp.float32)
    summed = lax.psum_scatter(
        partial_value.astype(jnp.bfloat16), "tp", scatter_dimension=3, tiled=True
    )
    returned = lax.all_to_all(summed, "ep", split_axis=0, concat_axis=0, tiled=True)
    results = returned.reshape(slot_count, returned.shape[3]).astype(jnp.float32)
    combined = jnp.dot(combine_rows, results, precision=lax.Precision.HIGHEST)
    local_squares = jnp.sum(combined * combined, axis=1)
    squares_all = lax.psum(local_squares, "tp")
    inverse_out = lax.rsqrt(squares_all / features + EPS)
    return (combined * inverse_out[:, None] * final_gain[None, :]).astype(jnp.bfloat16)


def fused_kernel(nz, tile, pieces, tokens_ref, gain_ref, routes_ref, rw_ref, wg_hbm, wu_hbm, wd_hbm, fgain_ref,
                 out_ref, buf, wg, wu, wd, hid, part, dbuf, xbuf, zbuf, total, meta, wsem,
                 az_s, az_r, ax_s, ax_r, ad_s, ad_r, md_s, md_r, rd_s, rd_r, rx_s, rx_r, rz_s, rz_r):
    rows, features = tokens_ref.shape
    hidden_units = wg.shape[1]
    experts = 4 * nz
    chunk = 4 * rows
    sub = rows // pieces
    halves, half = part.shape[1], part.shape[3]
    f32, bf16 = jnp.float32, jnp.bfloat16
    me = lax.axis_index("ep")
    core = lax.rem(me, 2)
    x = lax.rem(lax.div(me, 2), 2)
    z = lax.div(me, 4)
    d_peer = me + 1 - 2 * core
    x_peer = me + 2 - 4 * x
    has_below, has_above = z > 0, z < nz - 1
    inner = jnp.logical_and(has_below, has_above)
    outer = jnp.logical_not(inner)

    def weight_copy(which, j):
        src, dst = ((wg_hbm, wg), (wu_hbm, wu), (wd_hbm, wd))[which]
        cols = pl.ds(pl.multiple_of(j * tile, tile), tile)
        return pltpu.make_async_copy(src.at[0, :, cols], dst.at[:, cols], wsem.at[which, j])

    barrier = pltpu.get_barrier_semaphore()

    def greet(peer):
        pl.semaphore_signal(barrier, inc=1, device_id={"ep": peer}, device_id_type=MESH)

    greet(d_peer)
    greet(x_peer)
    pl.when(has_below)(lambda: greet(me - 4))
    pl.when(has_above)(lambda: greet(me + 4))

    gu_tiles, d_tiles = hidden_units // tile, features // tile
    for j in range(gu_tiles):
        weight_copy(0, j).start()
        weight_copy(1, j).start()
    for j in range(d_tiles):
        weight_copy(2, j).start()

    own = pl.ds(pl.multiple_of(me * rows, rows), rows)
    tok = tokens_ref[...].astype(f32)
    inverse = lax.rsqrt(jnp.mean(tok * tok, axis=1, keepdims=True) + EPS)
    buf[own, :] = (tok * inverse * gain_ref[...]).astype(bf16)
    lanes = lax.broadcasted_iota(jnp.int32, (experts, rows), 0)
    spread = jnp.zeros((experts, rows), f32)
    for k in range(routes_ref.shape[0]):
        spread = spread + jnp.where(lanes == routes_ref[k:k + 1, :], rw_ref[k:k + 1, :], 0.0)
    meta[me, :, :rows] = spread[:experts // 2]
    meta[me, :, rows:] = spread[experts // 2:]

    pl.semaphore_wait(barrier, jnp.where(inner, 4, 3))

    def remote(src, dst, s, r, dev):
        return pltpu.make_async_remote_copy(
            src_ref=src, dst_ref=dst, send_sem=s, recv_sem=r, device_id={"ep": dev}, device_id_type=MESH
        )

    own_step = nz - 1

    def order(q):
        rest = [p for p in range(nz) if p != q]
        if q in (0, nz - 1):
            return sorted(rest, key=lambda p: -abs(p - q))
        edge = 0 if 2 * q < nz else nz - 1
        return [edge] + sorted((p for p in rest if p != edge), key=lambda p: -abs(p - q))

    tables = [order(q) for q in range(nz)]
    places = []
    for i in range(own_step):
        value = tables[0][i]
        for q in range(1, nz):
            value = jnp.where(z == q, tables[q][i], value)
        places.append(value)
    places.append(z)

    def block_of(i, same_x, same_core):
        col = x if same_x else 1 - x
        lane = core if same_core else 1 - core
        return places[i] * 4 + col * 2 + lane

    def rows_of(i, same_x, same_core, q=None):
        at = block_of(i, same_x, same_core) * rows
        if q is None:
            return buf.at[pl.ds(pl.multiple_of(at, rows), rows), :]
        return buf.at[pl.ds(pl.multiple_of(at + q * sub, sub), sub), :]

    def piece(i, same_x, q):
        if q is META:
            return meta.at[block_of(i, same_x, True)]
        return rows_of(i, same_x, True, q)

    def slot_of(q):
        return pieces if q is META else q

    def ag_z(i, q, up):
        ref = piece(i, True, q)
        peer = me + 4 if up else me - 4
        return remote(ref, ref, az_s.at[i, int(up), slot_of(q)], az_r.at[places[i], slot_of(q)], peer)

    def ag_x(i, q, arriving=False):
        ref = piece(i, not arriving, q)
        return remote(ref, ref, ax_s.at[i, slot_of(q)], ax_r.at[i, slot_of(q)], x_peer)

    def ag_d(i, j, q):
        ref = piece(i, j == 0, q)
        s, r = (md_s, md_r) if q is META else (ad_s, ad_r)
        return remote(ref, ref, s.at[i, j], r.at[i, j], d_peer)

    def ag_d_all(i, j, arriving):
        ref = rows_of(i, j == 0, not arriving)
        return remote(ref, ref, ad_s.at[i, j], ad_r.at[i, j], d_peer)

    def meta_arrives(i, j):
        ref = meta.at[block_of(i, j == 0, False)]
        remote(ref, ref, md_s.at[i, j], md_r.at[i, j], d_peer).wait_recv()

    def start(copy):
        copy.start()

    def send_up(i, q, action):
        cond = has_above if i == own_step else jnp.logical_and(has_above, places[i] < z)
        pl.when(cond)(lambda: action(ag_z(i, q, True)))

    def send_down(i, q, action):
        cond = has_below if i == own_step else jnp.logical_and(has_below, places[i] > z)
        pl.when(cond)(lambda: action(ag_z(i, q, False)))

    def pass_on(i, q, action):
        send_up(i, q, action)
        send_down(i, q, action)

    def z_in(i, q):
        ag_z(i, q, True).wait_recv()
        pass_on(i, q, start)
        ag_d(i, 0, q).start()

    def x_out(i, q):
        ag_x(i, q).start()

    def x_in(i, q):
        ag_x(i, q, True).wait_recv()
        ag_d(i, 1, q).start()

    def rs_block(i, j, same_x, same_core):
        col = x if same_x else 1 - x
        lane = core if same_core else 1 - core
        at = pl.multiple_of((col * 2 + lane) * rows, rows)
        return part.at[i, j, pl.ds(at, rows), :]

    def rs_d(i, k, j):
        return remote(rs_block(i, j, k == 0, False), dbuf.at[i, k, j], rd_s.at[i, k, j], rd_r.at[i, k, j], d_peer)

    def rs_x(i, j):
        return remote(rs_block(i, j, False, True), xbuf.at[i, j], rx_s.at[i, j], rx_r.at[i, j], x_peer)

    def rs_z(i, j):
        up = places[i] > z
        slot = jnp.where(places[i] == z - 1, nz, places[i])
        peer = jnp.where(up, me + 4, me - 4)
        return remote(rs_block(i, j, True, True), zbuf.at[slot, j], rz_s.at[i, j], rz_r.at[slot, j], peer)

    def rs_z_arriving(slot, j):
        ref = zbuf.at[slot, j]
        return remote(ref, ref, rz_s.at[0, j], rz_r.at[slot, j], x_peer)

    def chunk_rows(i):
        return pl.ds(pl.multiple_of(places[i] * chunk, chunk), chunk)

    def gate_up(i, j):
        if i == own_step:
            weight_copy(0, j).wait()
            weight_copy(1, j).wait()
        cols = pl.ds(pl.multiple_of(j * tile, tile), tile)
        lhs = buf[chunk_rows(i), :]
        g = jnp.dot(lhs, wg[:, cols], preferred_element_type=f32)
        u = jnp.dot(lhs, wu[:, cols], preferred_element_type=f32)
        hid[:, cols] = (g / (1.0 + jnp.exp(-g)) * u).astype(bf16)

    def weight_of(i):
        eye = lax.broadcasted_iota(jnp.int32, (rows, rows), 0) == lax.broadcasted_iota(jnp.int32, (rows, rows), 1)
        line, side = lax.rem(me, experts // 2), lax.div(me, experts // 2)
        cols = []
        for b in range(4):
            both = meta[places[i] * 4 + b, pl.ds(line, 1), :]
            row = jnp.where(side == 0, both[:, :rows], both[:, rows:])
            cols.append(jnp.sum(jnp.where(eye, row, 0.0), axis=1, keepdims=True))
        return jnp.concatenate(cols, axis=0)

    def down(i):
        weight = weight_of(i)
        per = half // tile
        for j in range(halves):
            def body(t, carry):
                if i == own_step:
                    weight_copy(2, j * per + t).wait()
                cols = pl.ds(pl.multiple_of((j * per + t) * tile, tile), tile)
                o = jnp.dot(hid[...], wd[:, cols], preferred_element_type=f32)
                part[i, j, :, pl.ds(pl.multiple_of(t * tile, tile), tile)] = (o * weight).astype(bf16)
                return carry

            lax.fori_loop(0, per, body, 0)
            rs_d(i, 1, j).start()
            rs_d(i, 0, j).start()

    def finish_d(i, j):
        rs_d(i, 1, j).wait_recv()
        ref = rs_block(i, j, False, True)
        ref[...] = (ref[...].astype(f32) + dbuf[i, 1, j].astype(f32)).astype(bf16)
        rs_x(i, j).start()

    def finish_x(i, j):
        rs_d(i, 0, j).wait_recv()
        rs_x(i, j).wait_recv()
        ref = rs_block(i, j, True, True)
        value = ref[...].astype(f32) + dbuf[i, 0, j].astype(f32) + xbuf[i, j].astype(f32)
        if i == own_step:
            total[j] = value
        else:
            ref[...] = value.astype(bf16)
            pl.when(outer)(lambda: rs_z(i, j).start())

    def merge(i, j):
        rs_z_arriving(places[i], j).wait_recv()
        ref = rs_block(i, j, True, True)
        ref[...] = (ref[...].astype(f32) + zbuf[places[i], j].astype(f32)).astype(bf16)
        rs_z(i, j).start()

    def loop(i, duties):
        def body(j, carry):
            gate_up(i, j)
            duties(j)
            return carry

        lax.fori_loop(0, gu_tiles, body, 0)

    first = pieces // 2
    pass_on(own_step, META, start)
    x_out(own_step, META)
    ag_d(own_step, 0, META).start()
    for q in range(pieces):
        x_out(own_step, q)
        if q < first:
            pass_on(own_step, q, start)
        else:
            pl.when(outer)(lambda: pass_on(own_step, q, start))
        ag_d(own_step, 0, q).start()

    def late_inward(q):
        pl.when(2 * z < nz)(lambda: send_up(own_step, q, start))
        pl.when(2 * z >= nz)(lambda: send_down(own_step, q, start))

    def late_outward(q):
        pl.when(2 * z < nz)(lambda: send_down(own_step, q, start))
        pl.when(2 * z >= nz)(lambda: send_up(own_step, q, start))

    for q in range(first):
        x_in(own_step, q)

        @pl.when(inner)
        def _():
            z_in(0, q)
            x_out(0, q)
            z_in(2, q)

        @pl.when(outer)
        def _():
            z_in(2, q)
            x_out(2, q)

    for q in range(first, pieces):
        x_in(own_step, q)

        @pl.when(inner)
        def _():
            z_in(0, q)
            x_out(0, q)
            z_in(1, q - first)

        @pl.when(outer)
        def _():
            z_in(1, q - first)

    @pl.when(inner)
    def _():
        for q in range(first, pieces):
            late_inward(q)
        for q in range(first):
            x_out(1, q)
        z_in(0, META)
        x_out(0, META)

    x_in(own_step, META)
    z_in(2, META)
    x_out(2, META)
    ag_d_all(own_step, 0, True).wait_recv()
    ag_d_all(own_step, 1, True).wait_recv()

    def second_part(i, j):
        @pl.when(j < first)
        def _():
            z_in(i, j + first)
            x_out(i, j + first)

        @pl.when(j >= first)
        def _():
            z_in(2, j)

    def own_duties(j):
        @pl.when(inner)
        def _():
            second_part(1, j)

            @pl.when(j == first - 1)
            def _():
                for q in range(first, pieces):
                    late_outward(q)

        @pl.when(outer)
        def _():
            z_in(0, j)
            x_out(0, j)

        @pl.when(j >= 1)
        def _():
            x_in(0, j - 1)

    loop(own_step, own_duties)

    z_in(1, META)
    x_out(1, META)

    @pl.when(inner)
    def _():
        for q in range(pieces):
            x_out(2, q)

    @pl.when(outer)
    def _():
        for q in range(first):
            x_out(1, q)
        z_in(0, META)
        x_out(0, META)

    for j in range(2):
        meta_arrives(own_step, j)
    down(own_step)
    x_in(0, pieces - 1)
    for j in range(2):
        ag_d_all(0, j, True).wait_recv()

    def duties_0(j):
        @pl.when(outer)
        def _():
            second_part(1, j)
            pl.when(j >= first)(lambda: x_out(2, j))

        x_in(1, j)

    loop(0, duties_0)
    finish_d(own_step, 0)
    for i in range(own_step):
        x_in(i, META)
    for i in range(own_step):
        for j in range(2):
            meta_arrives(i, j)
    down(0)
    for j in range(2):
        ag_d_all(1, j, True).wait_recv()

    def duties_1(j):
        x_in(2, j)
        pl.when(j < halves)(lambda: finish_d(0, j))

    loop(1, duties_1)
    finish_x(own_step, 0)
    down(1)
    for j in range(2):
        ag_d_all(2, j, True).wait_recv()

    def duties_2(j):
        @pl.when(j < halves)
        def _():
            finish_d(1, j)
            finish_x(0, j)

    loop(2, duties_2)
    down(2)
    for j in range(halves):
        finish_d(2, j)
    finish_d(own_step, 1)
    for j in range(halves):
        finish_x(1, j)
        pl.when(inner)(lambda: merge(1, j))
    for j in range(halves):
        pl.when(inner)(lambda: merge(0, j))
    for j in range(halves):
        finish_x(2, j)
        pl.when(inner)(lambda: merge(2, j))
    finish_x(own_step, 1)

    @pl.when(has_below)
    def _():
        for j in range(halves):
            rs_z_arriving(z, j).wait_recv()
            total[j] = total[j] + zbuf[z, j].astype(f32)

    @pl.when(has_above)
    def _():
        for j in range(halves):
            rs_z_arriving(nz, j).wait_recv()
            total[j] = total[j] + zbuf[nz, j].astype(f32)

    squares = 0.0
    for j in range(halves):
        squares = squares + jnp.sum(total[j] * total[j], axis=1, keepdims=True)
    inverse_out = lax.rsqrt(squares / features + EPS)
    for j in range(halves):
        cols = pl.ds(j * half, half)
        out_ref[:, cols] = (total[j] * inverse_out * fgain_ref[:, cols]).astype(out_ref.dtype)

    for i in range(nz):
        for q in [META] + list(range(pieces)):
            pass_on(i, q, lambda copy: copy.wait_send())
            ag_x(i, q).wait_send()
        for j in range(2):
            ag_d(i, j, META).wait_send()
            ag_d_all(i, j, False).wait_send()
        for j in range(halves):
            rs_x(i, j).wait_send()
            for k in range(2):
                rs_d(i, k, j).wait_send()
            if i < own_step:
                rs_z(i, j).wait_send()


def fused_device(tokens, norm_gain, routes, route_weights, w_gate, w_up, w_down, final_gain):
    rows, features = tokens.shape
    hidden_units = w_gate.shape[2]
    experts = lax.axis_size("ep")
    nz = experts // 4
    pieces, halves = 4, 2
    tile = hidden_units // pieces
    half = features // halves
    vmem, anywhere = pl.BlockSpec(memory_space=pltpu.VMEM), pl.BlockSpec(memory_space=pl.ANY)
    dma = pltpu.SemaphoreType.DMA
    bf16 = jnp.bfloat16
    return pl.pallas_call(
        functools.partial(fused_kernel, nz, tile, pieces),
        out_shape=jax.ShapeDtypeStruct((rows, features), jnp.bfloat16),
        in_specs=[vmem, vmem, vmem, vmem, anywhere, anywhere, anywhere, vmem],
        out_specs=vmem,
        scratch_shapes=[
            pltpu.VMEM((experts * rows, features), bf16),
            pltpu.VMEM((features, hidden_units), bf16),
            pltpu.VMEM((features, hidden_units), bf16),
            pltpu.VMEM((hidden_units, features), bf16),
            pltpu.VMEM((4 * rows, hidden_units), bf16),
            pltpu.VMEM((nz, halves, 4 * rows, half), bf16),
            pltpu.VMEM((nz, 2, halves, rows, half), bf16),
            pltpu.VMEM((nz, halves, rows, half), bf16),
            pltpu.VMEM((nz + 1, halves, rows, half), bf16),
            pltpu.VMEM((halves, rows, half), jnp.float32),
            pltpu.VMEM((experts, experts // 2, 2 * rows), jnp.float32),
            dma((3, max(hidden_units, features) // tile)),
            dma((nz, 2, pieces + 1)), dma((nz, pieces + 1)), dma((nz, pieces + 1)), dma((nz, pieces + 1)),
            dma((nz, 2)), dma((nz, 2)), dma((nz, 2)), dma((nz, 2)),
            dma((nz, 2, halves)), dma((nz, 2, halves)), dma((nz, halves)), dma((nz, halves)),
            dma((nz, halves)), dma((nz + 1, halves)),
        ],
        compiler_params=pltpu.CompilerParams(
            collective_id=0, has_side_effects=True, vmem_limit_bytes=60 * 1024 * 1024
        ),
    )(tokens, norm_gain[None, :], routes.T, route_weights.T, w_gate, w_up, w_down, final_gain[None, :])


def solution(mesh):
    placed = (
        P(("grp", "ep"), None),
        P(),
        P(("grp", "ep"), None),
        P(("grp", "ep"), None),
        P("ep", None, "tp"),
        P("ep", None, "tp"),
        P("ep", "tp", None),
        P("tp"),
    )
    ep, tp = mesh.shape["ep"], mesh.shape["tp"]

    def step(*args):
        rows, features = args[0].shape
        hidden_units = args[4].shape[2]
        fits = 3 * features * hidden_units + 3 * ep * rows * features < 24 * 2 ** 20
        whole_tiles = features % 2048 == 0 and hidden_units % 2048 == 0 and rows % 64 == 0
        if tp == 1 and ep == 16 and args[4].shape[0] == 1 and fits and whole_tiles:
            return fused_device(*args)
        return per_device(*args)

    return jax.shard_map(
        step, mesh=mesh, in_specs=placed, out_specs=P(("grp", "ep"), "tp"), check_vma=False
    )
```

time: 82.7 us -> 74.8 us (0.904)
  Pallas kernels: 78 us -> 72.9 us
  local copies, waits for them, and re-layouts: 4.43 us -> 1.67 us
    pallas_call x1, Pallas kernels: 78 us -> 72.9 us  [fused_device(): pl.pallas_call(functools.partial(fused_kernel, nz, tile, pieces), out_sha...]
    unnamed x3 -> x1, local copies, waits for them, and re-layouts: 4.43 us -> 1.67 us
where the time goes in v1:
time: 74.8 us; the launch traced here: 74.5 us
  Pallas kernels  72.9 us (97%)
  local copies, waits for them, and re-layouts  1.67 us (2%)
    pallas_call x1, Pallas kernels, fused_device(): pl.pallas_call(functools.partial(fused_kernel, nz, tile, pieces), out_sha...  72.9 us
    unnamed x1, local copies, waits for them, and re-layouts  1.67 us

profile of v1, /device:TPU:0, one launch (start us, length us, event | category | flops | bytes accessed | tf_op | source)
XLA Modules:
  0.0 74.5 jit_solution(8953618675041690772)
XLA Ops:
  0.0 72.9 %shard_map.82 = bf16[64,2048]{1,0:T(8,128)(2,1)} custom-call(bf16[64,2048]{1,0:T(8,128)(2,1)} %tokens_ref.1, f32[1,2048]{1,0:T(1,128)} %bitcast.4, s32[6,64]{1,0:T(8,128)} %bitcast.6, f32[6,64]{1,0:T(8,128)} %bitcast.7, bf16[1,2048,2048]{2,1,0:T(8,128)(2,1)} %wg_hbm.1, bf16[1,2048,2048]{2,1,0:T(8,128)(2,1)} %wu_hbm.1, bf16[1,2048,2048]{2,1,0:T(8,128)(2,1)} %wd_hbm.1, ...), custom_call_target="tpu_custom_call" | custom-call | tf_op jit(solution)/shard_map/pallas_call | solution.py:511
  72.9 1.7 %copy.10 = bf16[64,2048]{1,0:T(8,128)(2,1)} copy(bf16[64,2048]{1,0:T(8,128)(2,1)} %shard_map.82) | data formatting | bytes 524288

commit v2 on v1

--- a/solution.py
+++ b/solution.py
@@ -60,7 +60,7 @@
 
 
 def fused_kernel(nz, tile, pieces, tokens_ref, gain_ref, routes_ref, rw_ref, wg_hbm, wu_hbm, wd_hbm, fgain_ref,
-                 out_ref, buf, wg, wu, wd, hid, part, dbuf, xbuf, zbuf, total, meta, wsem,
+                 out_ref, buf, wg, wu, wd, hid, hid_own, part, dbuf, xbuf, zbuf, total, meta, wsem,
                  az_s, az_r, ax_s, ax_r, ad_s, ad_r, md_s, md_r, rd_s, rd_r, rx_s, rx_r, rz_s, rz_r):
     rows, features = tokens_ref.shape
     hidden_units = wg.shape[1]
@@ -122,11 +122,12 @@
     own_step = nz - 1
 
     def order(q):
-        rest = [p for p in range(nz) if p != q]
-        if q in (0, nz - 1):
-            return sorted(rest, key=lambda p: -abs(p - q))
         edge = 0 if 2 * q < nz else nz - 1
-        return [edge] + sorted((p for p in rest if p != edge), key=lambda p: -abs(p - q))
+        far = nz - 1 - edge
+        if q == edge:
+            near = q + 1 if q == 0 else q - 1
+            return [near, far] + [p for p in range(nz) if p not in (q, near, far)]
+        return [p for p in range(nz) if p not in (q, edge, far)] + [far, edge]
 
     tables = [order(q) for q in range(nz)]
     places = []
@@ -218,9 +219,11 @@
         return remote(rs_block(i, j, False, True), xbuf.at[i, j], rx_s.at[i, j], rx_r.at[i, j], x_peer)
 
     def rs_z(i, j):
-        up = places[i] > z
-        slot = jnp.where(places[i] == z - 1, nz, places[i])
-        peer = jnp.where(up, me + 4, me - 4)
+        level, slot = places[i], z
+        if i == 1:
+            level = jnp.where(outer, jnp.where(has_below, z - 1, z + 1), level)
+            slot = jnp.where(outer, nz, slot)
+        peer = level * 4 + x * 2 + core
         return remote(rs_block(i, j, True, True), zbuf.at[slot, j], rz_s.at[i, j], rz_r.at[slot, j], peer)
 
     def rs_z_arriving(slot, j):
@@ -230,15 +233,23 @@
     def chunk_rows(i):
         return pl.ds(pl.multiple_of(places[i] * chunk, chunk), chunk)
 
+    def gate_up_rows(source, kept, target, j):
+        cols = pl.ds(pl.multiple_of(j * tile, tile), tile)
+        lhs = buf[source, :]
+        g = jnp.dot(lhs, wg[:, cols], preferred_element_type=f32)
+        u = jnp.dot(lhs, wu[:, cols], preferred_element_type=f32)
+        kept[target, cols] = (g / (1.0 + jnp.exp(-g)) * u).astype(bf16)
+
     def gate_up(i, j):
-        if i == own_step:
+        gate_up_rows(chunk_rows(i), hid, pl.ds(0, chunk), j)
+
+    def gate_up_chip(j, col, fresh):
+        if fresh:
             weight_copy(0, j).wait()
             weight_copy(1, j).wait()
-        cols = pl.ds(pl.multiple_of(j * tile, tile), tile)
-        lhs = buf[chunk_rows(i), :]
-        g = jnp.dot(lhs, wg[:, cols], preferred_element_type=f32)
-        u = jnp.dot(lhs, wu[:, cols], preferred_element_type=f32)
-        hid[:, cols] = (g / (1.0 + jnp.exp(-g)) * u).astype(bf16)
+        at = pl.multiple_of(col * (2 * rows), 2 * rows)
+        start_row = pl.multiple_of(z * chunk + col * (2 * rows), 2 * rows)
+        gate_up_rows(pl.ds(start_row, 2 * rows), hid_own, pl.ds(at, 2 * rows), j)
 
     def weight_of(i):
         eye = lax.broadcasted_iota(jnp.int32, (rows, rows), 0) == lax.broadcasted_iota(jnp.int32, (rows, rows), 1)
@@ -250,21 +261,22 @@
             cols.append(jnp.sum(jnp.where(eye, row, 0.0), axis=1, keepdims=True))
         return jnp.concatenate(cols, axis=0)
 
-    def down(i):
+    def down(i, duties):
         weight = weight_of(i)
-        per = half // tile
-        for j in range(halves):
-            def body(t, carry):
-                if i == own_step:
-                    weight_copy(2, j * per + t).wait()
-                cols = pl.ds(pl.multiple_of((j * per + t) * tile, tile), tile)
-                o = jnp.dot(hid[...], wd[:, cols], preferred_element_type=f32)
-                part[i, j, :, pl.ds(pl.multiple_of(t * tile, tile), tile)] = (o * weight).astype(bf16)
-                return carry
-
-            lax.fori_loop(0, per, body, 0)
-            rs_d(i, 1, j).start()
-            rs_d(i, 0, j).start()
+        kept = hid_own if i == own_step else hid
+
+        def body(t, carry):
+            if i == 0:
+                weight_copy(2, t).wait()
+            cols = pl.ds(pl.multiple_of(t * tile, tile), tile)
+            o = jnp.dot(kept[...], wd[:, cols], preferred_element_type=f32)
+            part[i, t] = (o * weight).astype(bf16)
+            rs_d(i, 1, t).start()
+            rs_d(i, 0, t).start()
+            duties(t)
+            return carry
+
+        lax.fori_loop(0, d_tiles, body, 0)
 
     def finish_d(i, j):
         rs_d(i, 1, j).wait_recv()
@@ -281,13 +293,12 @@
             total[j] = value
         else:
             ref[...] = value.astype(bf16)
-            pl.when(outer)(lambda: rs_z(i, j).start())
-
-    def merge(i, j):
-        rs_z_arriving(places[i], j).wait_recv()
-        ref = rs_block(i, j, True, True)
-        ref[...] = (ref[...].astype(f32) + zbuf[places[i], j].astype(f32)).astype(bf16)
-        rs_z(i, j).start()
+            if i == 1:
+                @pl.when(inner)
+                def _():
+                    rs_z_arriving(nz, j).wait_recv()
+                    ref[...] = (value + zbuf[nz, j].astype(f32)).astype(bf16)
+            rs_z(i, j).start()
 
     def loop(i, duties):
         def body(j, carry):
@@ -297,182 +308,166 @@
 
         lax.fori_loop(0, gu_tiles, body, 0)
 
-    first = pieces // 2
-    pass_on(own_step, META, start)
-    x_out(own_step, META)
-    ag_d(own_step, 0, META).start()
-    for q in range(pieces):
+    def chunk_ready(i):
+        for j in range(2):
+            ag_d_all(i, j, True).wait_recv()
+
+    def step(body):
+        lax.fori_loop(0, pieces, lambda j, carry: (body(j), carry)[1], 0)
+
+    for q in [META] + list(range(pieces)):
         x_out(own_step, q)
-        if q < first:
-            pass_on(own_step, q, start)
-        else:
-            pl.when(outer)(lambda: pass_on(own_step, q, start))
+        pass_on(own_step, q, start)
         ag_d(own_step, 0, q).start()
 
-    def late_inward(q):
-        pl.when(2 * z < nz)(lambda: send_up(own_step, q, start))
-        pl.when(2 * z >= nz)(lambda: send_down(own_step, q, start))
-
-    def late_outward(q):
-        pl.when(2 * z < nz)(lambda: send_down(own_step, q, start))
-        pl.when(2 * z >= nz)(lambda: send_up(own_step, q, start))
-
-    for q in range(first):
+    z_in(0, META)
+    x_out(0, META)
+
+    @pl.when(inner)
+    def _():
+        z_in(2, META)
+        x_out(2, META)
+
+    ag_d_all(own_step, 0, True).wait_recv()
+
+    def gather(q):
+        gate_up_chip(q, x, True)
         x_in(own_step, q)
+        z_in(0, q)
+        x_out(0, q)
+        pl.when(inner)(lambda: z_in(2, q))
+
+    step(gather)
+
+    @pl.when(inner)
+    def _():
+        z_in(1, META)
+        x_out(1, META)
+
+    @pl.when(outer)
+    def _():
+        z_in(2, META)
+        x_out(2, META)
+
+    ag_d_all(own_step, 1, True).wait_recv()
+
+    def own_rest(j):
+        gate_up_chip(j, 1 - x, False)
 
         @pl.when(inner)
         def _():
-            z_in(0, q)
-            x_out(0, q)
-            z_in(2, q)
+            z_in(1, j)
+            x_out(1, j)
 
         @pl.when(outer)
         def _():
-            z_in(2, q)
-            x_out(2, q)
-
-    for q in range(first, pieces):
-        x_in(own_step, q)
-
-        @pl.when(inner)
-        def _():
-            z_in(0, q)
-            x_out(0, q)
-            z_in(1, q - first)
-
-        @pl.when(outer)
-        def _():
-            z_in(1, q - first)
-
-    @pl.when(inner)
-    def _():
-        for q in range(first, pieces):
-            late_inward(q)
-        for q in range(first):
-            x_out(1, q)
-        z_in(0, META)
-        x_out(0, META)
-
-    x_in(own_step, META)
-    z_in(2, META)
-    x_out(2, META)
-    ag_d_all(own_step, 0, True).wait_recv()
-    ag_d_all(own_step, 1, True).wait_recv()
-
-    def second_part(i, j):
-        @pl.when(j < first)
-        def _():
-            z_in(i, j + first)
-            x_out(i, j + first)
-
-        @pl.when(j >= first)
-        def _():
             z_in(2, j)
-
-    def own_duties(j):
-        @pl.when(inner)
-        def _():
-            second_part(1, j)
-
-            @pl.when(j == first - 1)
-            def _():
-                for q in range(first, pieces):
-                    late_outward(q)
-
-        @pl.when(outer)
-        def _():
-            z_in(0, j)
-            x_out(0, j)
-
-        @pl.when(j >= 1)
-        def _():
-            x_in(0, j - 1)
-
-    loop(own_step, own_duties)
-
-    z_in(1, META)
-    x_out(1, META)
+            x_out(2, j)
+
+        x_in(0, j)
+
+    step(own_rest)
 
     @pl.when(inner)
     def _():
         for q in range(pieces):
             x_out(2, q)
 
+    x_in(own_step, META)
+    x_in(0, META)
+    chunk_ready(0)
+
+    def far_in(q):
+        z_in(1, q)
+        x_out(1, q)
+
+    def duties_0(j):
+        pl.when(outer)(lambda: far_in(j))
+        pl.when(inner)(lambda: x_in(1, j))
+
+    loop(0, duties_0)
+
     @pl.when(outer)
     def _():
-        for q in range(first):
-            x_out(1, q)
-        z_in(0, META)
-        x_out(0, META)
+        z_in(1, META)
+        x_out(1, META)
 
     for j in range(2):
-        meta_arrives(own_step, j)
-    down(own_step)
-    x_in(0, pieces - 1)
-    for j in range(2):
-        ag_d_all(0, j, True).wait_recv()
-
-    def duties_0(j):
-        @pl.when(outer)
-        def _():
-            second_part(1, j)
-            pl.when(j >= first)(lambda: x_out(2, j))
-
-        x_in(1, j)
-
-    loop(0, duties_0)
-    finish_d(own_step, 0)
-    for i in range(own_step):
-        x_in(i, META)
-    for i in range(own_step):
+        meta_arrives(0, j)
+
+    def down_duties_0(t):
+        pl.when(t >= 2)(lambda: finish_d(0, t - 2))
+        pl.when(outer)(lambda: x_in(1, t))
+
+    down(0, down_duties_0)
+    x_in(1, META)
+    x_in(2, META)
+    chunk_ready(1)
+
+    def duties_1(j):
+        pl.when(j < 2)(lambda: finish_d(0, j + 2))
+        x_in(2, j)
+        pl.when(j >= 2)(lambda: finish_x(0, j - 2))
+
+    loop(1, duties_1)
+    for i in range(1, nz):
         for j in range(2):
             meta_arrives(i, j)
-    down(0)
-    for j in range(2):
-        ag_d_all(1, j, True).wait_recv()
-
-    def duties_1(j):
-        x_in(2, j)
-        pl.when(j < halves)(lambda: finish_d(0, j))
-
-    loop(1, duties_1)
-    finish_x(own_step, 0)
-    down(1)
-    for j in range(2):
-        ag_d_all(2, j, True).wait_recv()
+
+    def down_duties_1(t):
+        @pl.when(t >= 2)
+        def _():
+            finish_d(1, t - 2)
+            finish_x(0, t)
+
+    down(1, down_duties_1)
+    chunk_ready(2)
 
     def duties_2(j):
-        @pl.when(j < halves)
-        def _():
-            finish_d(1, j)
-            finish_x(0, j)
+        pl.when(j < 2)(lambda: finish_d(1, j + 2))
+        pl.when(jnp.logical_and(j >= 2, outer))(lambda: finish_x(1, j - 2))
 
     loop(2, duties_2)
-    down(2)
-    for j in range(halves):
-        finish_d(2, j)
-    finish_d(own_step, 1)
-    for j in range(halves):
-        finish_x(1, j)
-        pl.when(inner)(lambda: merge(1, j))
-    for j in range(halves):
-        pl.when(inner)(lambda: merge(0, j))
-    for j in range(halves):
-        finish_x(2, j)
-        pl.when(inner)(lambda: merge(2, j))
-    finish_x(own_step, 1)
-
-    @pl.when(has_below)
-    def _():
-        for j in range(halves):
-            rs_z_arriving(z, j).wait_recv()
-            total[j] = total[j] + zbuf[z, j].astype(f32)
-
-    @pl.when(has_above)
-    def _():
-        for j in range(halves):
-            rs_z_arriving(nz, j).wait_recv()
-            total[j] = total[j] + zbuf[nz, j].astype(f32)
+
+    def down_duties_2(t):
+        pl.when(t >= 2)(lambda: finish_d(2, t - 2))
+        pl.when(jnp.logical_and(t < 2, outer))(lambda: finish_x(1, t + 2))
+
+    down(2, down_duties_2)
+
+    def down_duties_own(t):
+        pl.when(t < 2)(lambda: finish_d(2, t + 2))
+        pl.when(t >= 2)(lambda: finish_d(own_step, t - 2))
+        pl.when(inner)(lambda: finish_x(1, t))
+
+    down(own_step, down_duties_own)
+    finish_x(2, 0)
+    finish_d(own_step, 2)
+    finish_x(2, 1)
+    finish_d(own_step, 3)
+    finish_x(2, 2)
+    finish_x(2, 3)
+    for i in range(nz):
+        for q in [META] + list(range(pieces)):
+            pass_on(i, q, lambda copy: copy.wait_send())
+            ag_x(i, q).wait_send()
+        for j in range(2):
+            ag_d(i, j, META).wait_send()
+            ag_d_all(i, j, False).wait_send()
+    step(lambda j: finish_x(own_step, j))
+
+    def collect(level, cond):
+        def one(j):
+            rs_z_arriving(level, j).wait_recv()
+            total[j] = total[j] + zbuf[level, j].astype(f32)
+
+        pl.when(cond)(lambda: step(one))
+
+    for level in range(nz):
+        cond = z != level
+        if level in (0, nz - 1):
+            cond = jnp.logical_and(cond, inner)
+        collect(level, cond)
 
     squares = 0.0
     for j in range(halves):
@@ -483,12 +478,6 @@
         out_ref[:, cols] = (total[j] * inverse_out * fgain_ref[:, cols]).astype(out_ref.dtype)
 
     for i in range(nz):
-        for q in [META] + list(range(pieces)):
-            pass_on(i, q, lambda copy: copy.wait_send())
-            ag_x(i, q).wait_send()
-        for j in range(2):
-            ag_d(i, j, META).wait_send()
-            ag_d_all(i, j, False).wait_send()
         for j in range(halves):
             rs_x(i, j).wait_send()
             for k in range(2):
@@ -502,7 +491,7 @@
     hidden_units = w_gate.shape[2]
     experts = lax.axis_size("ep")
     nz = experts // 4
-    pieces, halves = 4, 2
+    pieces, halves = 4, 4
     tile = hidden_units // pieces
     half = features // halves
     vmem, anywhere = pl.BlockSpec(memory_space=pltpu.VMEM), pl.BlockSpec(memory_space=pl.ANY)
@@ -518,6 +507,7 @@
             pltpu.VMEM((features, hidden_units), bf16),
             pltpu.VMEM((features, hidden_units), bf16),
             pltpu.VMEM((hidden_units, features), bf16),
+            pltpu.VMEM((4 * rows, hidden_units), bf16),
             pltpu.VMEM((4 * rows, hidden_units), bf16),
             pltpu.VMEM((nz, halves, 4 * rows, half), bf16),
             pltpu.VMEM((nz, 2, halves, rows, half), bf16),

time: 74.8 us -> 66 us (0.88)
  Pallas kernels: 72.9 us -> 64.2 us
    pallas_call x1, Pallas kernels: 72.9 us -> 64.2 us  [fused_device(): pl.pallas_call(functools.partial(fused_kernel, nz, tile, pieces), out_sha...]
where the time goes in v2:
time: 66 us; the launch traced here: 65.8 us
  Pallas kernels  64.2 us (97%)
  local copies, waits for them, and re-layouts  1.67 us (3%)
    pallas_call x1, Pallas kernels, fused_device(): pl.pallas_call(functools.partial(fused_kernel, nz, tile, pieces), out_sha...  64.2 us
    unnamed x1, local copies, waits for them, and re-layouts  1.67 us

profile of v2, /device:TPU:0, one launch (start us, length us, event | category | flops | bytes accessed | tf_op | source)
XLA Modules:
  0.0 65.8 jit_solution(2318490523021531394)
XLA Ops:
  0.0 64.2 %shard_map.82 = bf16[64,2048]{1,0:T(8,128)(2,1)} custom-call(bf16[64,2048]{1,0:T(8,128)(2,1)} %tokens_ref.1, f32[1,2048]{1,0:T(1,128)} %bitcast.4, s32[6,64]{1,0:T(8,128)} %bitcast.6, f32[6,64]{1,0:T(8,128)} %bitcast.7, bf16[1,2048,2048]{2,1,0:T(8,128)(2,1)} %wg_hbm.1, bf16[1,2048,2048]{2,1,0:T(8,128)(2,1)} %wu_hbm.1, bf16[1,2048,2048]{2,1,0:T(8,128)(2,1)} %wd_hbm.1, ...), custom_call_target="tpu_custom_call" | custom-call | tf_op jit(solution)/shard_map/pallas_call | solution.py:500
  64.2 1.7 %copy.10 = bf16[64,2048]{1,0:T(8,128)(2,1)} copy(bf16[64,2048]{1,0:T(8,128)(2,1)} %shard_map.82) | data formatting | bytes 524288

commit v3 on v2

--- a/solution.py
+++ b/solution.py
@@ -61,13 +61,13 @@
 
 def fused_kernel(nz, tile, pieces, tokens_ref, gain_ref, routes_ref, rw_ref, wg_hbm, wu_hbm, wd_hbm, fgain_ref,
                  out_ref, buf, wg, wu, wd, hid, hid_own, part, dbuf, xbuf, zbuf, total, meta, wsem,
-                 az_s, az_r, ax_s, ax_r, ad_s, ad_r, md_s, md_r, rd_s, rd_r, rx_s, rx_r, rz_s, rz_r):
+                 sent, az_r, ax_r, ad_r, md_r, rd_r, rx_r, rz_r):
     rows, features = tokens_ref.shape
     hidden_units = wg.shape[1]
     experts = 4 * nz
     chunk = 4 * rows
     sub = rows // pieces
-    halves, half = part.shape[1], part.shape[3]
+    halves, half = part.shape[1], part.shape[5]
     f32, bf16 = jnp.float32, jnp.bfloat16
     me = lax.axis_index("ep")
     core = lax.rem(me, 2)
@@ -125,9 +125,8 @@
         edge = 0 if 2 * q < nz else nz - 1
         far = nz - 1 - edge
         if q == edge:
-            near = q + 1 if q == 0 else q - 1
-            return [near, far] + [p for p in range(nz) if p not in (q, near, far)]
-        return [p for p in range(nz) if p not in (q, edge, far)] + [far, edge]
+            return sorted((p for p in range(nz) if p != q), key=lambda p: abs(p - q))
+        return [edge] + [p for p in range(nz) if p not in (q, edge, far)] + [far]
 
     tables = [order(q) for q in range(nz)]
     places = []
@@ -160,24 +159,40 @@
     def ag_z(i, q, up):
         ref = piece(i, True, q)
         peer = me + 4 if up else me - 4
-        return remote(ref, ref, az_s.at[i, int(up), slot_of(q)], az_r.at[places[i], slot_of(q)], peer)
+        return remote(ref, ref, sent.at[int(up) + (2 if q is META else 0)], az_r.at[places[i], slot_of(q)], peer)
 
     def ag_x(i, q, arriving=False):
         ref = piece(i, not arriving, q)
-        return remote(ref, ref, ax_s.at[i, slot_of(q)], ax_r.at[i, slot_of(q)], x_peer)
+        return remote(ref, ref, sent.at[5 if q is META else 4], ax_r.at[i, slot_of(q)], x_peer)
 
     def ag_d(i, j, q):
         ref = piece(i, j == 0, q)
-        s, r = (md_s, md_r) if q is META else (ad_s, ad_r)
-        return remote(ref, ref, s.at[i, j], r.at[i, j], d_peer)
-
-    def ag_d_all(i, j, arriving):
-        ref = rows_of(i, j == 0, not arriving)
-        return remote(ref, ref, ad_s.at[i, j], ad_r.at[i, j], d_peer)
+        r = md_r if q is META else ad_r
+        return remote(ref, ref, sent.at[7 if q is META else 6], r.at[i, j], d_peer)
+
+    def ag_d_all(i, j):
+        ref = rows_of(i, j == 0, False)
+        return remote(ref, ref, sent.at[6], ad_r.at[i, j], d_peer)
 
     def meta_arrives(i, j):
         ref = meta.at[block_of(i, j == 0, False)]
-        remote(ref, ref, md_s.at[i, j], md_r.at[i, j], d_peer).wait_recv()
+        remote(ref, ref, sent.at[7], md_r.at[i, j], d_peer).wait_recv()
+
+    def sent_all(ref, n):
+        remote(ref, ref, sent.at[n], sent.at[n], d_peer).wait_send()
+
+    def gather_sent():
+        for k in range(nz):
+            @pl.when(z == k)
+            def _():
+                for up, blocks in ((0, nz - k if k > 0 else 0), (1, k + 1 if k < nz - 1 else 0)):
+                    if blocks:
+                        sent_all(buf.at[pl.ds(0, blocks * rows), :], up)
+                        sent_all(meta.at[pl.ds(0, blocks)], up + 2)
+        sent_all(buf.at[pl.ds(0, nz * rows), :], 4)
+        sent_all(meta.at[pl.ds(0, nz)], 5)
+        sent_all(buf.at[pl.ds(0, 2 * nz * rows), :], 6)
+        sent_all(meta.at[pl.ds(0, 2 * nz)], 7)
 
     def start(copy):
         copy.start()
@@ -206,42 +221,39 @@
         ag_x(i, q, True).wait_recv()
         ag_d(i, 1, q).start()
 
-    def rs_block(i, j, same_x, same_core):
-        col = x if same_x else 1 - x
-        lane = core if same_core else 1 - core
-        at = pl.multiple_of((col * 2 + lane) * rows, rows)
-        return part.at[i, j, pl.ds(at, rows), :]
-
-    def rs_d(i, k, j):
-        return remote(rs_block(i, j, k == 0, False), dbuf.at[i, k, j], rd_s.at[i, k, j], rd_r.at[i, k, j], d_peer)
+    def rs_block(i, j, same_x):
+        return part.at[i, j, x if same_x else 1 - x, core]
+
+    def rs_d(i, j):
+        return remote(part.at[i, j, :, 1 - core], dbuf.at[i, j], sent.at[8], rd_r.at[i, j], d_peer)
 
     def rs_x(i, j):
-        return remote(rs_block(i, j, False, True), xbuf.at[i, j], rx_s.at[i, j], rx_r.at[i, j], x_peer)
+        return remote(rs_block(i, j, False), xbuf.at[i, j], sent.at[9], rx_r.at[i, j], x_peer)
 
     def rs_z(i, j):
         level, slot = places[i], z
-        if i == 1:
-            level = jnp.where(outer, jnp.where(has_below, z - 1, z + 1), level)
-            slot = jnp.where(outer, nz, slot)
+        if i >= 1:
+            level = jnp.where(outer, places[0], level)
+            slot = jnp.where(outer, nz + i - 1, slot)
         peer = level * 4 + x * 2 + core
-        return remote(rs_block(i, j, True, True), zbuf.at[slot, j], rz_s.at[i, j], rz_r.at[slot, j], peer)
+        return remote(rs_block(i, j, True), zbuf.at[slot, j], sent.at[10], rz_r.at[slot, j], peer)
 
     def rs_z_arriving(slot, j):
         ref = zbuf.at[slot, j]
-        return remote(ref, ref, rz_s.at[0, j], rz_r.at[slot, j], x_peer)
+        return remote(ref, ref, sent.at[10], rz_r.at[slot, j], x_peer)
 
     def chunk_rows(i):
         return pl.ds(pl.multiple_of(places[i] * chunk, chunk), chunk)
 
-    def gate_up_rows(source, kept, target, j):
-        cols = pl.ds(pl.multiple_of(j * tile, tile), tile)
+    def gate_up_rows(source, kept, target, j, width):
+        cols = pl.ds(pl.multiple_of(j * width, width), width)
         lhs = buf[source, :]
         g = jnp.dot(lhs, wg[:, cols], preferred_element_type=f32)
         u = jnp.dot(lhs, wu[:, cols], preferred_element_type=f32)
         kept[target, cols] = (g / (1.0 + jnp.exp(-g)) * u).astype(bf16)
 
     def gate_up(i, j):
-        gate_up_rows(chunk_rows(i), hid, pl.ds(0, chunk), j)
+        gate_up_rows(chunk_rows(i), hid, pl.ds(0, chunk), j, 2 * tile)
 
     def gate_up_chip(j, col, fresh):
         if fresh:
@@ -249,7 +261,7 @@
             weight_copy(1, j).wait()
         at = pl.multiple_of(col * (2 * rows), 2 * rows)
         start_row = pl.multiple_of(z * chunk + col * (2 * rows), 2 * rows)
-        gate_up_rows(pl.ds(start_row, 2 * rows), hid_own, pl.ds(at, 2 * rows), j)
+        gate_up_rows(pl.ds(start_row, 2 * rows), hid_own, pl.ds(at, 2 * rows), j, tile)
 
     def weight_of(i):
         eye = lax.broadcasted_iota(jnp.int32, (rows, rows), 0) == lax.broadcasted_iota(jnp.int32, (rows, rows), 1)
@@ -261,43 +273,45 @@
             cols.append(jnp.sum(jnp.where(eye, row, 0.0), axis=1, keepdims=True))
         return jnp.concatenate(cols, axis=0)
 
-    def down(i, duties):
+    def down(i, duties, wide, begin=0, end=halves):
         weight = weight_of(i)
         kept = hid_own if i == own_step else hid
 
         def body(t, carry):
-            if i == 0:
-                weight_copy(2, t).wait()
-            cols = pl.ds(pl.multiple_of(t * tile, tile), tile)
+            cols = pl.ds(pl.multiple_of(t * wide * tile, wide * tile), wide * tile)
+            for n in range(wide):
+                if i == 0:
+                    weight_copy(2, t * wide + n).wait()
             o = jnp.dot(kept[...], wd[:, cols], preferred_element_type=f32)
-            part[i, t] = (o * weight).astype(bf16)
-            rs_d(i, 1, t).start()
-            rs_d(i, 0, t).start()
+            for n in range(wide):
+                value = (o[:, n * tile:(n + 1) * tile] * weight).astype(bf16)
+                part[i, t * wide + n] = value.reshape(2, 2, rows, half)
+            for n in range(wide):
+                rs_d(i, t * wide + n).start()
             duties(t)
             return carry
 
-        lax.fori_loop(0, d_tiles, body, 0)
+        lax.fori_loop(begin // wide, end // wide, body, 0)
 
     def finish_d(i, j):
-        rs_d(i, 1, j).wait_recv()
-        ref = rs_block(i, j, False, True)
-        ref[...] = (ref[...].astype(f32) + dbuf[i, 1, j].astype(f32)).astype(bf16)
+        rs_d(i, j).wait_recv()
+        ref = rs_block(i, j, False)
+        ref[...] = (ref[...].astype(f32) + dbuf[i, j, 1 - x].astype(f32)).astype(bf16)
         rs_x(i, j).start()
 
     def finish_x(i, j):
-        rs_d(i, 0, j).wait_recv()
         rs_x(i, j).wait_recv()
-        ref = rs_block(i, j, True, True)
-        value = ref[...].astype(f32) + dbuf[i, 0, j].astype(f32) + xbuf[i, j].astype(f32)
+        ref = rs_block(i, j, True)
+        value = ref[...].astype(f32) + dbuf[i, j, x].astype(f32) + xbuf[i, j].astype(f32)
         if i == own_step:
             total[j] = value
         else:
             ref[...] = value.astype(bf16)
-            if i == 1:
+            if i >= 1:
                 @pl.when(inner)
                 def _():
-                    rs_z_arriving(nz, j).wait_recv()
-                    ref[...] = (value + zbuf[nz, j].astype(f32)).astype(bf16)
+                    rs_z_arriving(nz + i - 1, j).wait_recv()
+                    ref[...] = (value + zbuf[nz + i - 1, j].astype(f32)).astype(bf16)
             rs_z(i, j).start()
 
     def loop(i, duties):
@@ -306,11 +320,11 @@
             duties(j)
             return carry
 
-        lax.fori_loop(0, gu_tiles, body, 0)
+        lax.fori_loop(0, gu_tiles // 2, body, 0)
 
     def chunk_ready(i):
         for j in range(2):
-            ag_d_all(i, j, True).wait_recv()
+            ag_d_all(i, j).wait_recv()
 
     def step(body):
         lax.fori_loop(0, pieces, lambda j, carry: (body(j), carry)[1], 0)
@@ -325,135 +339,131 @@
 
     @pl.when(inner)
     def _():
-        z_in(2, META)
-        x_out(2, META)
-
-    ag_d_all(own_step, 0, True).wait_recv()
+        z_in(1, META)
+        x_out(1, META)
+
+    ag_d_all(own_step, 0).wait_recv()
 
     def gather(q):
         gate_up_chip(q, x, True)
         x_in(own_step, q)
         z_in(0, q)
         x_out(0, q)
-        pl.when(inner)(lambda: z_in(2, q))
+        pl.when(inner)(lambda: z_in(1, q))
 
     step(gather)
 
     @pl.when(inner)
+    def _():
+        z_in(2, META)
+        x_out(2, META)
+
+    @pl.when(outer)
     def _():
         z_in(1, META)
         x_out(1, META)
+
+    ag_d_all(own_step, 1).wait_recv()
+
+    def own_rest(j):
+        gate_up_chip(j, 1 - x, False)
+        pl.when(inner)(lambda: z_in(2, j))
+        pl.when(outer)(lambda: z_in(1, j))
+        x_out(1, j)
+        x_in(0, j)
+
+    step(own_rest)
+
+    @pl.when(inner)
+    def _():
+        for q in range(pieces):
+            x_out(2, q)
 
     @pl.when(outer)
     def _():
         z_in(2, META)
         x_out(2, META)
 
-    ag_d_all(own_step, 1, True).wait_recv()
-
-    def own_rest(j):
-        gate_up_chip(j, 1 - x, False)
-
-        @pl.when(inner)
-        def _():
-            z_in(1, j)
-            x_out(1, j)
-
-        @pl.when(outer)
-        def _():
-            z_in(2, j)
-            x_out(2, j)
-
-        x_in(0, j)
-
-    step(own_rest)
-
-    @pl.when(inner)
-    def _():
-        for q in range(pieces):
-            x_out(2, q)
-
     x_in(own_step, META)
     x_in(0, META)
     chunk_ready(0)
 
+    def both(action, j):
+        action(2 * j)
+        action(2 * j + 1)
+
     def far_in(q):
-        z_in(1, q)
-        x_out(1, q)
+        z_in(2, q)
+        x_out(2, q)
 
     def duties_0(j):
-        pl.when(outer)(lambda: far_in(j))
-        pl.when(inner)(lambda: x_in(1, j))
+        pl.when(outer)(lambda: both(far_in, j))
+
+        @pl.when(j == 0)
+        def _():
+            x_in(1, 0)
+
+        @pl.when(j == 1)
+        def _():
+            x_in(1, 1)
+            x_in(1, 2)
 
     loop(0, duties_0)
-
-    @pl.when(outer)
-    def _():
-        z_in(1, META)
-        x_out(1, META)
-
     for j in range(2):
         meta_arrives(0, j)
 
     def down_duties_0(t):
-        pl.when(t >= 2)(lambda: finish_d(0, t - 2))
-        pl.when(outer)(lambda: x_in(1, t))
-
-    down(0, down_duties_0)
+        pl.when(t == 0)(lambda: x_in(1, 3))
+        pl.when(t == 1)(lambda: both(lambda j: finish_d(0, j), 0))
+
+    down(0, down_duties_0, 2)
     x_in(1, META)
+    chunk_ready(1)
+
+    def duties_1(j):
+        pl.when(j == 0)(lambda: both(lambda q: finish_d(0, q), 1))
+        both(lambda q: x_in(2, q), j)
+
+    loop(1, duties_1)
     x_in(2, META)
-    chunk_ready(1)
-
-    def duties_1(j):
-        pl.when(j < 2)(lambda: finish_d(0, j + 2))
-        x_in(2, j)
-        pl.when(j >= 2)(lambda: finish_x(0, j - 2))
-
-    loop(1, duties_1)
-    for i in range(1, nz):
+    for j in range(2):
+        meta_arrives(1, j)
+
+    def down_duties_1(t):
+        pl.when(t == 1)(lambda: both(lambda j: finish_d(1, j), 0))
+        both(lambda j: finish_x(0, j), t)
+
+    down(1, down_duties_1, 2)
+    chunk_ready(2)
+
+    def duties_2(j):
+        pl.when(j == 0)(lambda: both(lambda q: finish_d(1, q), 1))
+        pl.when(jnp.logical_and(j == 1, outer))(lambda: finish_x(1, 0))
+
+    loop(2, duties_2)
+    for i in (2, own_step):
         for j in range(2):
             meta_arrives(i, j)
 
-    def down_duties_1(t):
-        @pl.when(t >= 2)
-        def _():
-            finish_d(1, t - 2)
-            finish_x(0, t)
-
-    down(1, down_duties_1)
-    chunk_ready(2)
-
-    def duties_2(j):
-        pl.when(j < 2)(lambda: finish_d(1, j + 2))
-        pl.when(jnp.logical_and(j >= 2, outer))(lambda: finish_x(1, j - 2))
-
-    loop(2, duties_2)
-
     def down_duties_2(t):
         pl.when(t >= 2)(lambda: finish_d(2, t - 2))
-        pl.when(jnp.logical_and(t < 2, outer))(lambda: finish_x(1, t + 2))
-
-    down(2, down_duties_2)
+        pl.when(jnp.logical_and(t < 3, outer))(lambda: finish_x(1, t + 1))
+
+    down(2, down_duties_2, 1)
 
     def down_duties_own(t):
         pl.when(t < 2)(lambda: finish_d(2, t + 2))
         pl.when(t >= 2)(lambda: finish_d(own_step, t - 2))
         pl.when(inner)(lambda: finish_x(1, t))
 
-    down(own_step, down_duties_own)
+    down(own_step, down_duties_own, 1)
     finish_x(2, 0)
     finish_d(own_step, 2)
     finish_x(2, 1)
     finish_d(own_step, 3)
     finish_x(2, 2)
     finish_x(2, 3)
-    for i in range(nz):
-        for q in [META] + list(range(pieces)):
-            pass_on(i, q, lambda copy: copy.wait_send())
-            ag_x(i, q).wait_send()
-        for j in range(2):
-            ag_d(i, j, META).wait_send()
-            ag_d_all(i, j, False).wait_send()
+    gather_sent()
     step(lambda j: finish_x(own_step, j))
 
     def collect(level, cond):
@@ -464,10 +474,10 @@
         pl.when(cond)(lambda: step(one))
 
     for level in range(nz):
-        cond = z != level
         if level in (0, nz - 1):
-            cond = jnp.logical_and(cond, inner)
-        collect(level, cond)
+            collect(level, z == (1 if level == 0 else nz - 2))
+        else:
+            collect(level, z != level)
 
     squares = 0.0
     for j in range(halves):
@@ -477,13 +487,9 @@
         cols = pl.ds(j * half, half)
         out_ref[:, cols] = (total[j] * inverse_out * fgain_ref[:, cols]).astype(out_ref.dtype)
 
-    for i in range(nz):
-        for j in range(halves):
-            rs_x(i, j).wait_send()
-            for k in range(2):
-                rs_d(i, k, j).wait_send()
-            if i < own_step:
-                rs_z(i, j).wait_send()
+    sent_all(dbuf, 8)
+    sent_all(xbuf, 9)
+    sent_all(zbuf.at[pl.ds(0, own_step)], 10)
 
 
 def fused_device(tokens, norm_gain, routes, route_weights, w_gate, w_up, w_down, final_gain):
@@ -509,17 +515,15 @@
             pltpu.VMEM((hidden_units, features), bf16),
             pltpu.VMEM((4 * rows, hidden_units), bf16),
             pltpu.VMEM((4 * rows, hidden_units), bf16),
-            pltpu.VMEM((nz, halves, 4 * rows, half), bf16),
-            pltpu.VMEM((nz, 2, halves, rows, half), bf16),
+            pltpu.VMEM((nz, halves, 2, 2, rows, half), bf16),
+            pltpu.VMEM((nz, halves, 2, rows, half), bf16),
             pltpu.VMEM((nz, halves, rows, half), bf16),
-            pltpu.VMEM((nz + 1, halves, rows, half), bf16),
+            pltpu.VMEM((nz + 2, halves, rows, half), bf16),
             pltpu.VMEM((halves, rows, half), jnp.float32),
             pltpu.VMEM((experts, experts // 2, 2 * rows), jnp.float32),
             dma((3, max(hidden_units, features) // tile)),
-            dma((nz, 2, pieces + 1)), dma((nz, pieces + 1)), dma((nz, pieces + 1)), dma((nz, pieces + 1)),
-            dma((nz, 2)), dma((nz, 2)), dma((nz, 2)), dma((nz, 2)),
-            dma((nz, 2, halves)), dma((nz, 2, halves)), dma((nz, halves)), dma((nz, halves)),
-            dma((nz, halves)), dma((nz + 1, halves)),
+            dma((11,)), dma((nz, pieces + 1)), dma((nz, pieces + 1)), dma((nz, 2)), dma((nz, 2)),
+            dma((nz, halves)), dma((nz, halves)), dma((nz + 2, halves)),
         ],
         compiler_params=pltpu.CompilerParams(
             collective_id=0, has_side_effects=True, vmem_limit_bytes=60 * 1024 * 1024

time: 66 us -> 62.8 us (0.952)
  Pallas kernels: 64.2 us -> 60.9 us
    pallas_call x1, Pallas kernels: 64.2 us -> 60.9 us  [fused_device(): pl.pallas_call(functools.partial(fused_kernel, nz, tile, pieces), out_sha...]
where the time goes in v3:
time: 62.8 us; the launch traced here: 62.6 us
  Pallas kernels  60.9 us (97%)
  local copies, waits for them, and re-layouts  1.67 us (3%)
    pallas_call x1, Pallas kernels, fused_device(): pl.pallas_call(functools.partial(fused_kernel, nz, tile, pieces), out_sha...  60.9 us
    unnamed x1, local copies, waits for them, and re-layouts  1.67 us

profile of v3, /device:TPU:0, one launch (start us, length us, event | category | flops | bytes accessed | tf_op | source)
XLA Modules:
  0.0 62.6 jit_solution(17800314795919590168)
XLA Ops:
  0.0 60.9 %shard_map.82 = bf16[64,2048]{1,0:T(8,128)(2,1)} custom-call(bf16[64,2048]{1,0:T(8,128)(2,1)} %tokens_ref.1, f32[1,2048]{1,0:T(1,128)} %bitcast.4, s32[6,64]{1,0:T(8,128)} %bitcast.6, f32[6,64]{1,0:T(8,128)} %bitcast.7, bf16[1,2048,2048]{2,1,0:T(8,128)(2,1)} %wg_hbm.1, bf16[1,2048,2048]{2,1,0:T(8,128)(2,1)} %wu_hbm.1, bf16[1,2048,2048]{2,1,0:T(8,128)(2,1)} %wd_hbm.1, ...), custom_call_target="tpu_custom_call" | custom-call | tf_op jit(solution)/shard_map/pallas_call | solution.py:506
  60.9 1.7 %copy.10 = bf16[64,2048]{1,0:T(8,128)(2,1)} copy(bf16[64,2048]{1,0:T(8,128)(2,1)} %shard_map.82) | data formatting | bytes 524288

commit v4 on v3

--- a/solution.py
+++ b/solution.py
@@ -59,8 +59,8 @@
     return (combined * inverse_out[:, None] * final_gain[None, :]).astype(jnp.bfloat16)
 
 
-def fused_kernel(nz, tile, pieces, tokens_ref, gain_ref, routes_ref, rw_ref, wg_hbm, wu_hbm, wd_hbm, fgain_ref,
-                 out_ref, buf, wg, wu, wd, hid, hid_own, part, dbuf, xbuf, zbuf, total, meta, wsem,
+def fused_kernel(nz, tile, pieces, tokens_hbm, gain_hbm, routes_hbm, rw_hbm, wg_hbm, wu_hbm, wd_hbm, fgain_hbm,
+                 out_ref, tokens_ref, gain_ref, routes_ref, rw_ref, fgain_ref, small, buf, wg, wu, wd, hid, hid_own, part, dbuf, xbuf, zbuf, total, meta, wsem,
                  sent, az_r, ax_r, ad_r, md_r, rd_r, rx_r, rz_r):
     rows, features = tokens_ref.shape
     hidden_units = wg.shape[1]
@@ -94,13 +94,25 @@
     pl.when(has_below)(lambda: greet(me - 4))
     pl.when(has_above)(lambda: greet(me + 4))
 
+    loads = [
+        pltpu.make_async_copy(src, dst, small.at[n])
+        for n, (src, dst) in enumerate((
+            (tokens_hbm, tokens_ref), (gain_hbm, gain_ref), (routes_hbm, routes_ref), (rw_hbm, rw_ref),
+            (fgain_hbm, fgain_ref),
+        ))
+    ]
+    for load in loads:
+        load.start()
+
     gu_tiles, d_tiles = hidden_units // tile, features // tile
     for j in range(gu_tiles):
-        weight_copy(0, j).start()
-        weight_copy(1, j).start()
+        weight_copy(0, j).start(priority=1)
+        weight_copy(1, j).start(priority=1)
     for j in range(d_tiles):
-        weight_copy(2, j).start()
-
+        weight_copy(2, j).start(priority=1)
+
+    for load in loads:
+        load.wait()
     own = pl.ds(pl.multiple_of(me * rows, rows), rows)
     tok = tokens_ref[...].astype(f32)
     inverse = lax.rsqrt(jnp.mean(tok * tok, axis=1, keepdims=True) + EPS)
@@ -414,14 +426,13 @@
 
     def down_duties_0(t):
         pl.when(t == 0)(lambda: x_in(1, 3))
-        pl.when(t == 1)(lambda: both(lambda j: finish_d(0, j), 0))
 
     down(0, down_duties_0, 2)
     x_in(1, META)
     chunk_ready(1)
 
     def duties_1(j):
-        pl.when(j == 0)(lambda: both(lambda q: finish_d(0, q), 1))
+        both(lambda q: finish_d(0, q), j)
         both(lambda q: x_in(2, q), j)
 
     loop(1, duties_1)
@@ -431,13 +442,17 @@
 
     def down_duties_1(t):
         pl.when(t == 1)(lambda: both(lambda j: finish_d(1, j), 0))
-        both(lambda j: finish_x(0, j), t)
+        pl.when(t == 1)(lambda: both(lambda j: finish_x(0, j), 0))
 
     down(1, down_duties_1, 2)
     chunk_ready(2)
 
     def duties_2(j):
-        pl.when(j == 0)(lambda: both(lambda q: finish_d(1, q), 1))
+        @pl.when(j == 0)
+        def _():
+            both(lambda q: finish_d(1, q), 1)
+            both(lambda q: finish_x(0, q), 1)
+
         pl.when(jnp.logical_and(j == 1, outer))(lambda: finish_x(1, 0))
 
     loop(2, duties_2)
@@ -500,15 +515,21 @@
     pieces, halves = 4, 4
     tile = hidden_units // pieces
     half = features // halves
-    vmem, anywhere = pl.BlockSpec(memory_space=pltpu.VMEM), pl.BlockSpec(memory_space=pl.ANY)
+    vmem, hbm = pl.BlockSpec(memory_space=pltpu.VMEM), pl.BlockSpec(memory_space=pltpu.HBM)
     dma = pltpu.SemaphoreType.DMA
     bf16 = jnp.bfloat16
     return pl.pallas_call(
         functools.partial(fused_kernel, nz, tile, pieces),
         out_shape=jax.ShapeDtypeStruct((rows, features), jnp.bfloat16),
-        in_specs=[vmem, vmem, vmem, vmem, anywhere, anywhere, anywhere, vmem],
+        in_specs=[hbm] * 8,
         out_specs=vmem,
         scratch_shapes=[
+            pltpu.VMEM((rows, features), bf16),
+            pltpu.VMEM((1, features), jnp.float32),
+            pltpu.VMEM(routes.shape[::-1], jnp.int32),
+            pltpu.VMEM(routes.shape[::-1], jnp.float32),
+            pltpu.VMEM((1, features), jnp.float32),
+            dma((5,)),
             pltpu.VMEM((experts * rows, features), bf16),
             pltpu.VMEM((features, hidden_units), bf16),
             pltpu.VMEM((features, hidden_units), bf16),
@@ -526,9 +547,14 @@
             dma((nz, halves)), dma((nz, halves)), dma((nz + 2, halves)),
         ],
         compiler_params=pltpu.CompilerParams(
-            collective_id=0, has_side_effects=True, vmem_limit_bytes=60 * 1024 * 1024
+            collective_id=0, has_side_effects=True, vmem_limit_bytes=48 * 1024 * 1024
         ),
-    )(tokens, norm_gain[None, :], routes.T, route_weights.T, w_gate, w_up, w_down, final_gain[None, :])
+    )(*(
+        pltpu.with_memory_space_constraint(array, pltpu.HBM)
+        for array in (
+            tokens, norm_gain[None, :], routes.T, route_weights.T, w_gate, w_up, w_down, final_gain[None, :],
+        )
+    ))
 
 
 def solution(mesh):

time: 62.8 us -> 60.8 us (0.968)
  Pallas kernels: 60.9 us -> 59.9 us
  local copies, waits for them, and re-layouts: 1.67 us -> 0.71 us
    pallas_call x1, Pallas kernels: 60.9 us -> 59.9 us  [fused_device(): pl.pallas_call(functools.partial(fused_kernel, nz, tile, pieces), out_sha...]
    unnamed x1, local copies, waits for them, and re-layouts: 1.67 us -> 0.71 us
where the time goes in v4:
time: 60.8 us; the launch traced here: 60.6 us
  Pallas kernels  59.9 us (99%)
  local copies, waits for them, and re-layouts  0.71 us (1%)
    pallas_call x1, Pallas kernels, fused_device(): pl.pallas_call(functools.partial(fused_kernel, nz, tile, pieces), out_sha...  59.9 us

profile of v4, /device:TPU:0, one launch (start us, length us, event | category | flops | bytes accessed | tf_op | source)
XLA Modules:
  0.0 60.6 jit_solution(1146563274495810459)
XLA Ops:
  0.0 59.9 %shard_map.82 = bf16[64,2048]{1,0:T(8,128)(2,1)S(1)} custom-call(bf16[64,2048]{1,0:T(8,128)(2,1)} %tokens_hbm.1, f32[1,2048]{1,0:T(1,128)} %bitcast.4, s32[6,64]{1,0:T(8,128)} %bitcast.6, f32[6,64]{1,0:T(8,128)} %bitcast.7, bf16[1,2048,2048]{2,1,0:T(8,128)(2,1)} %wg_hbm.1, bf16[1,2048,2048]{2,1,0:T(8,128)(2,1)} %wu_hbm.1, bf16[1,2048,2048]{2,1,0:T(8,128)(2,1)} %wd_hbm.1, ...), custom_call_target="tpu_custom_call" | custom-call | tf_op jit(solution)/shard_map/pallas_call | solution.py:521
  59.9 0.7 %copy.10 = bf16[64,2048]{1,0:T(8,128)(2,1)} copy(bf16[64,2048]{1,0:T(8,128)(2,1)S(1)} %shard_map.82) | data formatting | bytes 524288

commit v5 on v4

--- a/solution.py
+++ b/solution.py
@@ -267,13 +267,13 @@
     def gate_up(i, j):
         gate_up_rows(chunk_rows(i), hid, pl.ds(0, chunk), j, 2 * tile)
 
-    def gate_up_chip(j, col, fresh):
+    def gate_up_chip(j, col, fresh, i=own_step):
         if fresh:
             weight_copy(0, j).wait()
             weight_copy(1, j).wait()
         at = pl.multiple_of(col * (2 * rows), 2 * rows)
-        start_row = pl.multiple_of(z * chunk + col * (2 * rows), 2 * rows)
-        gate_up_rows(pl.ds(start_row, 2 * rows), hid_own, pl.ds(at, 2 * rows), j, tile)
+        start_row = pl.multiple_of(places[i] * chunk + col * (2 * rows), 2 * rows)
+        gate_up_rows(pl.ds(start_row, 2 * rows), hid_own if i == own_step else hid, pl.ds(at, 2 * rows), j, tile)
 
     def weight_of(i):
         eye = lax.broadcasted_iota(jnp.int32, (rows, rows), 0) == lax.broadcasted_iota(jnp.int32, (rows, rows), 1)
@@ -383,6 +383,8 @@
         pl.when(outer)(lambda: z_in(1, j))
         x_out(1, j)
         x_in(0, j)
+        pl.when(j == 0)(lambda: ag_d_all(0, 0).wait_recv())
+        gate_up_chip(j, x, False, 0)
 
     step(own_rest)
 
@@ -398,7 +400,7 @@
 
     x_in(own_step, META)
     x_in(0, META)
-    chunk_ready(0)
+    ag_d_all(0, 1).wait_recv()
 
     def both(action, j):
         action(2 * j)
@@ -408,19 +410,12 @@
         z_in(2, q)
         x_out(2, q)
 
-    def duties_0(j):
-        pl.when(outer)(lambda: both(far_in, j))
-
-        @pl.when(j == 0)
-        def _():
-            x_in(1, 0)
-
-        @pl.when(j == 1)
-        def _():
-            x_in(1, 1)
-            x_in(1, 2)
-
-    loop(0, duties_0)
+    def near_rest(j):
+        gate_up_chip(j, 1 - x, False, 0)
+        pl.when(outer)(lambda: far_in(j))
+        pl.when(j >= 1)(lambda: x_in(1, j - 1))
+
+    step(near_rest)
     for j in range(2):
         meta_arrives(0, j)
 

time: 60.8 us -> 59.8 us (0.984)
  Pallas kernels: 59.9 us -> 58.9 us
    pallas_call x1, Pallas kernels: 59.9 us -> 58.9 us  [fused_device(): pl.pallas_call(functools.partial(fused_kernel, nz, tile, pieces), out_sha...]
where the time goes in v5:
time: 59.8 us; the launch traced here: 59.6 us
  Pallas kernels  58.9 us (98%)
  local copies, waits for them, and re-layouts  0.71 us (1%)
    pallas_call x1, Pallas kernels, fused_device(): pl.pallas_call(functools.partial(fused_kernel, nz, tile, pieces), out_sha...  58.9 us

profile of v5, /device:TPU:0, one launch (start us, length us, event | category | flops | bytes accessed | tf_op | source)
XLA Modules:
  0.0 59.6 jit_solution(12877426114049894091)
XLA Ops:
  0.0 58.9 %shard_map.82 = bf16[64,2048]{1,0:T(8,128)(2,1)S(1)} custom-call(bf16[64,2048]{1,0:T(8,128)(2,1)} %tokens_hbm.1, f32[1,2048]{1,0:T(1,128)} %bitcast.4, s32[6,64]{1,0:T(8,128)} %bitcast.6, f32[6,64]{1,0:T(8,128)} %bitcast.7, bf16[1,2048,2048]{2,1,0:T(8,128)(2,1)} %wg_hbm.1, bf16[1,2048,2048]{2,1,0:T(8,128)(2,1)} %wu_hbm.1, bf16[1,2048,2048]{2,1,0:T(8,128)(2,1)} %wd_hbm.1, ...), custom_call_target="tpu_custom_call" | custom-call | tf_op jit(solution)/shard_map/pallas_call | solution.py:516
  58.9 0.7 %copy.10 = bf16[64,2048]{1,0:T(8,128)(2,1)} copy(bf16[64,2048]{1,0:T(8,128)(2,1)S(1)} %shard_map.82) | data formatting | bytes 524288
